TPU v7x, 32 devices: a whole 2x2x4 slice. The times are simulated.
32 devices in a mesh: tp: 32 (over z, y, x, core).
Axes of the slice: x: 2, y: 2, z: 4, core: 2. Of those that a mesh axis runs over, the one named last changes fastest.
Arguments:
- tokens: bfloat16 [32, 4096], replicated, may hold values from -18 to 18
- norm_gain: float32 [2, 4096], replicated, may hold values from 0.1 to 1.9
- w_gate: bfloat16 [2, 4096, 8192], P(None, None, 'tp'), may hold values from -0.09375 to 0.09375
- w_value: bfloat16 [2, 4096, 8192], P(None, None, 'tp'), may hold values from -0.09375 to 0.09375
- w_write: bfloat16 [2, 4096, 1024], P(None, None, 'tp'), may hold values from -0.09375 to 0.09375
- w_read: bfloat16 [2, 4096, 1024], P(None, None, 'tp'), may hold values from -0.09375 to 0.09375
- w_step: bfloat16 [2, 4096, 128], replicated, may hold values from -0.09375 to 0.09375
- step_bias: float32 [2, 128], replicated, may hold values from -2 to 1
- decay_rate: float32 [2, 128], replicated, may hold values from 0.05 to 3
- skip_gain: float32 [2, 128], replicated, may hold values from 1 to 4
- conv_value_weight: float32 [2, 3, 8192], P(None, None, 'tp'), may hold values from -2.5 to 2.5
- conv_key_weight: float32 [2, 3, 2, 1024], P(None, None, None, 'tp'), may hold values from -2.5 to 2.5
- group_gain: float32 [2, 8192], P(None, 'tp'), may hold values from 0.1 to 1.9
- w_out: bfloat16 [2, 8192, 4096], P(None, 'tp'), may hold values from -0.0625 to 0.0625
- ssm_state: float32 [2, 32, 8192, 128], P(None, None, 'tp'), may hold values from -3 to 3
- conv_value: float32 [2, 32, 2, 8192], P(None, None, None, 'tp'), may hold values from -5 to 5
- conv_key: float32 [2, 32, 2, 2, 1024], P(None, None, None, None, 'tp'), may hold values from -5 to 5
Outputs:
- tokens_out: bfloat16 [32, 4096], replicated
- ssm_state_out: float32 [2, 32, 8192, 128], P(None, None, 'tp')
- conv_value_out: float32 [2, 32, 2, 8192], P(None, None, None, 'tp')
- conv_key_out: float32 [2, 32, 2, 2, 1024], P(None, None, None, None, 'tp')
All inputs are finite; a program needn't handle non-finite values.
Results may differ from a plain program's by a relative error of at most 0.011.
Values may be sent and summed in bfloat16 or wider, within the bound.
A program may use at most 128 MiB of HBM per device.

v0:
```python
import jax
import jax.numpy as jnp
from jax import lax
from jax.sharding import PartitionSpec as P

D = 4096
HEAD_DIM = 64
GROUPS = 8
STATE = 128
LAYERS = 2
HEADS = 128
GW = 1024


EPS = 1e-06


def per_device(
    tokens,
    norm_gain,
    w_gate,
    w_value,
    w_write,
    w_read,
    w_step,
    step_bias,
    decay_rate,
    skip_gain,
    conv_value_weight,
    conv_key_weight,
    group_gain,
    w_out,
    ssm_state,
    conv_value,
    conv_key,
):
    highest = lax.Precision.HIGHEST
    chan_count = w_gate.shape[2]
    position = lax.axis_index("tp")
    first_chan = position * chan_count
    chan_ids = first_chan + jnp.arange(chan_count, dtype=jnp.int32)
    my_group = first_chan // GW
    head_hot = (
        (chan_ids // HEAD_DIM)[:, None] == jnp.arange(HEADS, dtype=jnp.int32)[None, :]
    ).astype(jnp.float32)
    group_hot = ((chan_ids // GW)[:, None] == jnp.arange(GROUPS, dtype=jnp.int32)[None, :]).astype(
        jnp.float32
    )
    hidden = tokens
    ssm_list = []
    value_list = []
    key_list = []
    for layer in range(LAYERS):
        resid = hidden.astype(jnp.float32)
        inv_scale = lax.rsqrt(jnp.sum(resid * resid, axis=1) / D + EPS)[:, None]
        scaled = (resid * norm_gain[layer]).astype(jnp.bfloat16)

        def project(weight):
            return jnp.dot(scaled, weight[layer], preferred_element_type=jnp.float32) * inv_scale

        gate_in = project(w_gate)
        value_in = project(w_value)
        write_in = project(w_write)
        read_in = project(w_read)
        step_in = project(w_step)
        value_window = jnp.concatenate([conv_value[layer], value_in[:, None, :]], axis=1)
        value_list.append(value_window[:, 1:])
        values = jax.nn.silu(jnp.sum(value_window * conv_value_weight[layer][None], axis=1))
        fresh = jnp.stack([write_in, read_in], axis=1)[:, None]
        key_window = jnp.concatenate([conv_key[layer], fresh], axis=1)
        key_list.append(key_window[:, 1:])
        mixed_keys = jax.nn.silu(jnp.sum(key_window * conv_key_weight[layer][None], axis=1))
        every_group = lax.all_gather(mixed_keys, "tp", axis=2, tiled=True)
        by_entry = every_group.reshape(every_group.shape[0], 2, STATE, GROUPS)
        own_keys = lax.dynamic_slice_in_dim(by_entry, my_group, 1, 3)[..., 0]
        writes = own_keys[:, 0]
        reads = own_keys[:, 1]
        delta = jax.nn.softplus(step_in + step_bias[layer][None])
        decay = jnp.exp(-delta * decay_rate[layer][None])
        delta_chan = jnp.dot(delta, head_hot.T, precision=highest)
        decay_chan = jnp.dot(decay, head_hot.T, precision=highest)
        skip_chan = jnp.dot(skip_gain[layer], head_hot.T, precision=highest)
        state = (
            decay_chan[..., None] * ssm_state[layer]
            + (delta_chan * values)[..., None] * writes[:, None, :]
        )
        ssm_list.append(state)
        read_out = jnp.sum(state * reads[:, None, :], axis=2) + skip_chan[None] * values
        gated = read_out * jax.nn.silu(gate_in)
        squares = jnp.dot(gated * gated, group_hot, precision=highest)
        square_total = lax.psum(squares, "tp")
        group_scale = lax.rsqrt(square_total / GW + EPS)
        scale_chan = jnp.dot(group_scale, group_hot.T, precision=highest)
        normed = (gated * scale_chan * group_gain[layer][None]).astype(jnp.bfloat16)
        partial_out = jnp.dot(normed, w_out[layer], preferred_element_type=jnp.float32)
        update = lax.psum(partial_out, "tp")
        hidden = (resid + update).astype(jnp.bfloat16)
    return (hidden, jnp.stack(ssm_list), jnp.stack(value_list), jnp.stack(key_list))


def solution(mesh):
    placed = (
        P(),
        P(),
        P(None, None, "tp"),
        P(None, None, "tp"),
        P(None, None, "tp"),
        P(None, None, "tp"),
        P(),
        P(),
        P(),
        P(),
        P(None, None, "tp"),
        P(None, None, None, "tp"),
        P(None, "tp"),
        P(None, "tp", None),
        P(None, None, "tp", None),
        P(None, None, None, "tp"),
        P(None, None, None, None, "tp"),
    )
    return jax.shard_map(
        per_device,
        mesh=mesh,
        in_specs=placed,
        out_specs=(
            P(),
            P(None, None, "tp", None),
            P(None, None, None, "tp"),
            P(None, None, None, None, "tp"),
        ),
        check_vma=False,
    )
```

profile of v0, /device:TPU:0, one launch (start us, length us, event | category | flops | bytes accessed | tf_op | source)
XLA Modules:
  0.0 486.0 jit_solution(18059725305354858468)
XLA Ops:
  7.2 0.0 all-reduce.3.cloned.1.call-start
  7.3 1.3 fusion.57
  8.6 0.8 slice_bitcast_fusion.11
  9.3 0.8 slice_bitcast_fusion.10
  10.1 0.8 fusion.160
  10.9 0.8 fusion.159
  11.6 0.7 slice_bitcast_fusion.8
  12.3 0.9 fusion.158
  13.2 1.2 fusion.51
  14.4 1.2 fusion.50
  15.8 2.1 fusion.29
  18.0 0.1 fusion.77
  18.1 0.0 copy-done.5
  18.1 0.3 compare_select_fusion.1
  18.4 0.3 fusion.79
  18.7 0.1 fusion.73
  18.8 0.3 convolution_multiply_fusion.3
  19.1 0.1 fusion.92
  19.3 0.1 copy.61
  19.3 46.2 %all_gather.6 = f32[32,2,1024]{0,1,2:T(2,128)S(1)} all-gather(f32[32,2,32]{0,1,2:T(2,128)S(1)} %copy.61), channel_id=1, replica_groups=mesh['tp'=32] {'tp'}, dimensions={2}, use_global_device_ids=true | all-gather | bytes 270336 | tf_op jit(solution)/shard_map/all_gather | solution.py:73
  65.5 0.1 copy.80
  65.6 0.1 constant_dynamic-slice_fusion.1
  65.7 0.1 copy.63
  65.8 5.5 %fusion.5 = f32[32,256]{1,0:T(8,128)S(1)} fusion(f32[2,32,256,128]{3,2,1,0:T(8,128)} %param.31, f32[32,128]{1,0:T(8,128)S(1)} %get-tuple-element.17, f32[32,128]{1,0:T(8,128)S(1)} %get-tuple-element.16, f32[32,256]{1,0:T(8,128)S(1)} %convolution_multiply_fusion.3, f32[32,256]{1,0:T(8,128)S(1)} %fusion.79), kind=kLoop, calls=%fused_computation.8 | loop fusion | flops 5234688 | bytes 4325376 | tf_op jit(solution)/shard_map/reduce_sum | solution.py:88
  71.3 0.0 copy-start.6
  71.4 0.4 multiply_multiply_fusion.1
  71.8 0.3 fusion.75
  72.1 36.8 %psum.28 = f32[32,8]{0,1:T(8,128)S(1)} all-reduce(f32[32,8]{0,1:T(8,128)S(1)} %fusion.75), channel_id=1, replica_groups=mesh['tp'=32] {'tp'}, use_global_device_ids=true, to_apply=%region_4.5 | all-reduce | flops 256 | bytes 2048 | tf_op jit(solution)/shard_map/psum | solution.py:91
  108.9 0.3 fusion.44
  109.2 2.9 fusion.12
  112.1 0.0 all-reduce.3.cloned.1.call-update
  112.1 0.0 all-reduce.5.cloned.1.call-start
  112.2 0.1 fusion.101
  112.3 0.1 fusion.76
  112.4 129.4 %all-reduce.3.cloned.1.call-done = f32[32,4096]{1,0:T(8,128)} async-done(((f32[32,4096]{1,0:T(8,128)}), f32[32,4096]{1,0:T(8,128)}) %all-reduce.3.cloned.1.call-update) | async-done | bytes 524304 | tf_op jit(solution)/shard_map/psum | solution.py:96
  241.8 1.2 fusion.60
  243.0 0.2 fusion.48
  243.2 0.0 copy-done.7
  243.3 0.2 fusion.49
  243.5 2.0 fusion.38
  245.5 1.5 compare_select_fusion
  247.1 0.1 fusion.93
  247.3 0.1 copy.68
  247.4 0.1 fusion.99
  247.5 0.1 fusion.71
  247.6 0.3 fusion.78
  247.9 0.3 convolution_multiply_fusion.1
  248.1 42.5 %all_gather.7 = f32[32,2,1024]{0,1,2:T(2,128)S(1)} all-gather(f32[32,2,32]{0,1,2:T(2,128)S(1)} %copy.68), channel_id=1, replica_groups=mesh['tp'=32] {'tp'}, dimensions={2}, use_global_device_ids=true | all-gather | bytes 270336 | tf_op jit(solution)/shard_map/all_gather | solution.py:73
  290.6 0.1 copy.79
  290.7 0.1 constant_dynamic-slice_fusion
  290.8 0.1 copy.70
  290.9 10.5 %multiply_add_fusion.1 = (f32[1,32,256,128]{3,2,1,0:T(8,128)}, f32[1,32,256,128]{3,2,1,0:T(8,128)}) fusion(f32[2,32,256,128]{3,2,1,0:T(8,128)} %param.31, f32[32,128]{1,0:T(8,128)S(1)} %get-tuple-element.16, f32[32,256]{1,0:T(8,128)S(1)} %convolution_multiply_fusion.3, f32[32,256]{1,0:T(8,128)S(1)} %fusion.79, f32[32,128]{1,0:T(8,128)S(1)} %get-tuple-element.12, ...), kind=kLoop, calls=%fused_computation.10 | loop fusion | flops 6291456 | bytes 16941056 | tf_op jit(solution)/shard_map/add | solution.py:84
  301.4 5.5 %fusion.2 = f32[32,256]{1,0:T(8,128)S(1)} fusion(f32[2,32,256,128]{3,2,1,0:T(8,128)} %param.31, f32[32,128]{1,0:T(8,128)S(1)} %get-tuple-element.13, f32[32,128]{1,0:T(8,128)S(1)} %get-tuple-element.12, f32[32,256]{1,0:T(8,128)S(1)} %convolution_multiply_fusion.1, f32[32,256]{1,0:T(8,128)S(1)} %fusion.78), kind=kLoop, calls=%fused_computation.4 | loop fusion | flops 5234688 | bytes 4325376 | tf_op jit(solution)/shard_map/reduce_sum | solution.py:88
  306.9 0.4 multiply_multiply_fusion
  307.3 0.3 fusion.74
  307.6 36.8 %psum.30 = f32[32,8]{0,1:T(8,128)S(1)} all-reduce(f32[32,8]{0,1:T(8,128)S(1)} %fusion.74), channel_id=1, replica_groups=mesh['tp'=32] {'tp'}, use_global_device_ids=true, to_apply=%region_10.11 | all-reduce | flops 256 | bytes 2048 | tf_op jit(solution)/shard_map/psum | solution.py:91
  344.5 0.3 fusion.45
  344.7 2.9 fusion.6
  347.7 0.0 all-reduce.5.cloned.1.call-update
  347.7 0.7 pad_maximum_fusion.4
  348.4 0.7 pad_maximum_fusion.3
  349.1 7.9 %pad_maximum_fusion = f32[2,32,256,128]{3,2,1,0:T(8,128)} fusion(f32[1,32,256,128]{3,2,1,0:T(8,128)} %get-tuple-element.7, f32[1,32,256,128]{3,2,1,0:T(8,128)} %get-tuple-element.6), kind=kLoop, calls=%fused_computation | loop fusion | flops 2097152 | bytes 16777216 | tf_op jit(solution)/shard_map/stack | solution.py:98
  357.0 120.4 %all-reduce.5.cloned.1.call-done = f32[32,4096]{1,0:T(8,128)} async-done(((f32[32,4096]{1,0:T(8,128)}), f32[32,4096]{1,0:T(8,128)}) %all-reduce.5.cloned.1.call-update) | async-done | bytes 524304 | tf_op jit(solution)/shard_map/psum | solution.py:96
  477.4 1.8 fusion.61
  (34 shorter events, 0.4 us)
Async XLA Ops:
  7.2 10.9 %copy-start = (bf16[32,4096]{1,0:T(8,128)(2,1)S(1)}, bf16[32,4096]{1,0:T(8,128)(2,1)}, u32[]{:S(2)}) copy-start(bf16[32,4096]{1,0:T(8,128)(2,1)} %param.17) | copy-start | bytes 786436
  7.2 10.7 %copy-start.1 = (f32[2,32,2,256]{3,2,1,0:T(2,128)S(1)}, f32[2,32,2,256]{3,2,1,0:T(2,128)}, u32[]{:S(2)}) copy-start(f32[2,32,2,256]{3,2,1,0:T(2,128)} %param.32) | copy-start | bytes 393220
  7.2 10.8 %copy-start.8 = (f32[2,128]{1,0:T(2,128)S(1)}, f32[2,128]{1,0:T(2,128)}, u32[]{:S(2)}) copy-start(f32[2,128]{1,0:T(2,128)} %param.26) | copy-start | bytes 3076
  7.2 11.9 %copy-start.2 = (f32[2,32,2,2,32]{4,3,2,1,0:T(2,128)S(1)}, f32[2,32,2,2,32]{4,3,2,1,0:T(2,128)}, u32[]{:S(2)}) copy-start(f32[2,32,2,2,32]{4,3,2,1,0:T(2,128)} %param.33) | copy-start | bytes 98308
  7.2 234.6 %all-reduce.3.cloned.1.call-start = ((), (), s32[]{:S(2)}) async-start(), calls=%async_computation | async-start | bytes 1048576 | tf_op jit(solution)/shard_map/psum | solution.py:96
  7.3 10.8 %copy-start.5 = (bf16[2,4096,128]{2,1,0:T(8,128)(2,1)S(1)}, bf16[2,4096,128]{2,1,0:T(8,128)(2,1)}, u32[]{:S(2)}) copy-start(bf16[2,4096,128]{2,1,0:T(8,128)(2,1)} %param.23) | copy-start | bytes 6291460
  65.8 5.6 %copy-start.3 = (bf16[2,4096,256]{2,1,0:T(8,128)(2,1)S(1)}, bf16[2,4096,256]{2,1,0:T(8,128)(2,1)}, u32[]{:S(2)}) copy-start(bf16[2,4096,256]{2,1,0:T(8,128)(2,1)} %param.19) | copy-start | bytes 12582916
  71.3 171.7 %copy-start.6 = (bf16[2,4096,32]{1,2,0:T(8,128)(2,1)S(1)}, bf16[2,4096,32]{1,2,0:T(8,128)(2,1)}, u32[]{:S(2)}) copy-start(bf16[2,4096,32]{1,2,0:T(8,128)(2,1)} %param.22) | copy-start | bytes 1572868
  71.3 171.9 %copy-start.7 = (bf16[2,4096,32]{1,2,0:T(8,128)(2,1)S(1)}, bf16[2,4096,32]{1,2,0:T(8,128)(2,1)}, u32[]{:S(2)}) copy-start(bf16[2,4096,32]{1,2,0:T(8,128)(2,1)} %param.21) | copy-start | bytes 1572868
  112.1 365.3 %all-reduce.5.cloned.1.call-start = ((), (), s32[]{:S(2)}) async-start(), calls=%async_computation.1 | async-start | bytes 1048576 | tf_op jit(solution)/shard_map/psum | solution.py:96
  301.4 5.5 %copy-start.4 = (bf16[2,4096,256]{2,1,0:T(8,128)(2,1)S(1)}, bf16[2,4096,256]{2,1,0:T(8,128)(2,1)}, u32[]{:S(2)}) copy-start(bf16[2,4096,256]{2,1,0:T(8,128)(2,1)} %param.19) | copy-start | bytes 12582916
Sparse Core Ops, SparseCore 0:
  112.2 129.5 all-reduce.2
  347.8 129.4 all-reduce.4
where the time goes:
time: 487 us; the launch traced here: 486 us
  waiting for transfers between devices  250 us (51%)
  blocking collectives  162 us (33%)
  other arithmetic  35.8 us (7%)
  matrix products  18 us (4%)
  between operations  14.5 us (3%)
  local copies, waits for them, and re-layouts  5.49 us (1%)
    psum x2, waiting for transfers between devices, per_device(): update = lax.psum(partial_out, 'tp')  250 us
    all_gather x2, blocking collectives, per_device(): every_group = lax.all_gather(mixed_keys, 'tp', axis=2, tiled=True)  88.7 us
    psum x2, blocking collectives, per_device(): square_total = lax.psum(squares, 'tp')  73.6 us
    reduce_sum x2, other arithmetic, per_device(): jnp.sum(state * reads[:, None, :], axis=2) + skip_chan[None] * values  11 us
    add x1, other arithmetic, per_device(): decay_chan[..., None] * ssm_state[layer]  10.5 us
  transfers between devices with their start and end apart: 2, of which 2 were waited for; matrix products, arithmetic and copies ran while one was open for 2% of the time, Pallas kernels for 0%

commit v1 on v0

--- a/solution.py
+++ b/solution.py
@@ -1,7 +1,10 @@
 import jax
 import jax.numpy as jnp
 from jax import lax
+from jax.experimental import pallas as pl
+from jax.experimental.pallas import tpu as pltpu
 from jax.sharding import PartitionSpec as P
+import functools
 
 D = 4096
 HEAD_DIM = 64
@@ -98,6 +101,500 @@
     return (hidden, jnp.stack(ssm_list), jnp.stack(value_list), jnp.stack(key_list))
 
 
+LANES = 128
+TAPS = 3
+BF16 = jnp.bfloat16
+F32 = jnp.float32
+NT = (((1,), (1,)), ((), ()))
+
+
+def split3(x):
+    high = x.astype(BF16)
+    rest = x - high.astype(F32)
+    mid = rest.astype(BF16)
+    return high, mid, (rest - mid.astype(F32)).astype(BF16)
+
+
+def select_dot(x, hot):
+    rows = x.shape[0]
+    parts = jnp.concatenate(split3(x), axis=0)
+    out = jnp.dot(parts, hot, preferred_element_type=F32)
+    return out[:rows] + out[rows : 2 * rows] + out[2 * rows :]
+
+
+def silu(v):
+    return v / (1.0 + jnp.exp(-v))
+
+
+def iota(shape, axis):
+    return lax.broadcasted_iota(jnp.int32, shape, axis)
+
+
+def kernel(
+    n,
+    tokens_hbm,
+    gain_hbm,
+    wg_hbm,
+    wv_hbm,
+    ww_hbm,
+    wr_hbm,
+    ws_hbm,
+    bias_hbm,
+    rate_hbm,
+    skip_hbm,
+    cvw_hbm,
+    ckw_hbm,
+    gg_hbm,
+    wo_hbm,
+    state_hbm,
+    cv_hbm,
+    ck_hbm,
+    tokens_out,
+    state_out,
+    value_out,
+    write_out,
+    read_out_ref,
+    tokens,
+    gain,
+    wg,
+    wv,
+    ww,
+    wr,
+    ws,
+    bias,
+    rate,
+    skip,
+    cvw,
+    ckw,
+    gg,
+    wo,
+    state,
+    cv,
+    ck,
+    hidden,
+    scaled,
+    keys_send,
+    keys_recv,
+    sq_send,
+    sq_recv,
+    part,
+    rs_send,
+    rs_recv,
+    cols,
+    wbuf,
+    rbuf,
+    qbuf,
+    in_small,
+    in_big,
+    out_sem,
+    key_ss,
+    key_rs,
+    sq_ss,
+    sq_rs,
+    rs_ss,
+    rs_rs,
+    ag_ss,
+    ag_rs,
+):
+    layers, batch, chans, entries = state.shape
+    width = hidden.shape[3]
+    depth = tokens.shape[1]
+    key_cols = ww.shape[2]
+    own_entries = key_cols // GROUPS
+    span = 2 * own_entries
+    heads = bias.shape[1]
+    peers = GW // chans
+    me = lax.axis_index("tp")
+    my_group = me // peers
+    first = my_group * peers
+    kstep = 512
+    ksteps = depth // kstep
+
+    small_pairs = (
+        (tokens_hbm, tokens),
+        (gain_hbm, gain),
+        (bias_hbm, bias),
+        (rate_hbm, rate),
+        (skip_hbm, skip),
+        (cvw_hbm, cvw),
+        (ckw_hbm, ckw),
+        (gg_hbm, gg),
+        (cv_hbm, cv),
+        (ck_hbm, ck),
+    )
+    small = [pltpu.make_async_copy(a, b, in_small.at[i]) for i, (a, b) in enumerate(small_pairs)]
+    big = [
+        [
+            pltpu.make_async_copy(a.at[l], b.at[l], in_big.at[l, i])
+            for i, (a, b) in enumerate(
+                (
+                    (ww_hbm, ww),
+                    (wr_hbm, wr),
+                    (wg_hbm, wg),
+                    (wv_hbm, wv),
+                    (ws_hbm, ws),
+                    (state_hbm, state),
+                    (wo_hbm, wo),
+                )
+            )
+        ]
+        for l in range(layers)
+    ]
+    for copy in small[:2] + big[0][:2] + small[2:] + big[0][2:] + big[1]:
+        copy.start()
+
+    barrier = pltpu.get_barrier_semaphore()
+
+    def greet(k, carry):
+        pl.semaphore_signal(
+            barrier,
+            inc=1,
+            device_id=(lax.rem(me + k, n),),
+            device_id_type=pl.DeviceIdType.MESH,
+        )
+        return carry
+
+    lax.fori_loop(1, n, greet, 0)
+
+    def remote(src, dst, ss, rs, to):
+        return pltpu.make_async_remote_copy(
+            src_ref=src,
+            dst_ref=dst,
+            send_sem=ss,
+            recv_sem=rs,
+            device_id=(to,),
+            device_id_type=pl.DeviceIdType.MESH,
+        )
+
+    def key_copy(l, k, slot):
+        to = lax.rem(me + k, n)
+        return remote(
+            keys_send.at[l, to // peers], keys_recv.at[l, slot], key_ss.at[l, k], key_rs.at[l, k], to
+        )
+
+    def rs_copy(l, k, slot):
+        to = lax.rem(me + k, n)
+        return remote(rs_send.at[l, to], rs_recv.at[l, slot], rs_ss.at[l, k], rs_rs.at[l, k], to)
+
+    def ag_copy(l, k, slot):
+        to = lax.rem(me + k, n)
+        return remote(
+            hidden.at[l, me], hidden.at[l, slot], ag_ss.at[l, k], ag_rs.at[l, k], to
+        )
+
+    def sq_copy(l, k):
+        to = first + lax.rem(me - first + k, peers)
+        return remote(
+            sq_send.at[l], sq_recv.at[l, k], sq_ss.at[l, k], sq_rs.at[l, k], to
+        )
+
+    def each(body):
+        def step(k, carry):
+            body(k)
+            return carry
+
+        lax.fori_loop(1, n, step, 0)
+
+    def came_from(k):
+        return lax.rem(me + n - k, n)
+
+    row = iota((2 * key_cols, key_cols), 0)
+    col = iota((2 * key_cols, key_cols), 1)
+    source = (row % own_entries) * GROUPS + row // span
+    is_read = (row % span) // own_entries
+    send_hot = [
+        jnp.where((col == source) & (is_read == i), 1.0, 0.0).astype(BF16) for i in range(2)
+    ]
+    row = iota((n * span, 2 * entries), 0)
+    col = iota((n * span, 2 * entries), 1)
+    target = ((row % span) // own_entries) * entries + (row // span) * own_entries + row % own_entries
+    recv_hot = jnp.where(col == target, 1.0, 0.0).astype(BF16)
+    row = iota((heads, chans), 0)
+    col = iota((heads, chans), 1)
+    head_hot = jnp.where(row == (me * chans + col) // HEAD_DIM, 1.0, 0.0).astype(BF16)
+
+    def update_state(l, group):
+        turned = pltpu.roll(cols[...], lax.rem(LANES - 8 * group, LANES), 1)
+        writes8 = wbuf[pl.ds(pl.multiple_of(8 * group, 8), 8), :]
+        for j in range(8):
+            b = 8 * group + j
+            state[l, b] = (
+                turned[:, batch + j : batch + j + 1] * state[l, b]
+                + turned[:, j : j + 1] * writes8[j : j + 1, :]
+            )
+        pltpu.make_async_copy(
+            state.at[l, pl.ds(8 * group, 8)],
+            state_out.at[l, pl.ds(8 * group, 8)],
+            out_sem.at[l, group],
+        ).start()
+
+    groups8 = batch // 8
+
+    def update_range(l, low, high):
+        def step(g, carry):
+            update_state(l, g)
+            return carry
+
+        lax.fori_loop(low, high, step, 0)
+
+    for copy in small[:2]:
+        copy.wait()
+
+    for l in range(layers):
+        if l == 0:
+            def piece(j):
+                return tokens[:, j * width : (j + 1) * width]
+        else:
+            def piece(j):
+                return hidden[l - 1, j]
+        squares = jnp.zeros((batch, width), F32)
+        for j in range(n):
+            x = piece(j).astype(F32)
+            squares = squares + x * x
+            scaled[:, j * width : (j + 1) * width] = (
+                x * gain[l : l + 1, j * width : (j + 1) * width]
+            ).astype(BF16)
+        inv_scale = lax.rsqrt(jnp.sum(squares, axis=1, keepdims=True) / depth + EPS)
+
+        def project(refs):
+            def step(k, accs):
+                at = pl.ds(pl.multiple_of(k * kstep, kstep), kstep)
+                x = scaled[:, at]
+                return tuple(
+                    acc + jnp.dot(x, ref[l, at, :], preferred_element_type=F32)
+                    for acc, ref in zip(accs, refs)
+                )
+
+            zeros = tuple(jnp.zeros((batch, ref.shape[2]), F32) for ref in refs)
+            return [acc * inv_scale for acc in lax.fori_loop(0, ksteps, step, zeros)]
+
+        big[l][0].wait()
+        big[l][1].wait()
+        write_in, read_in = project((ww, wr))
+        write_out[l] = write_in
+        read_out_ref[l] = read_in
+        if l == 0:
+            for copy in small[2:]:
+                copy.wait()
+        keys_t = jnp.zeros((2 * key_cols, LANES), F32)
+        for i, fresh in enumerate((write_in, read_in)):
+            mixed = fresh * ckw[l, TAPS - 1, i : i + 1, :]
+            for k in range(TAPS - 1):
+                mixed = mixed + ck[l, k, i] * ckw[l, k, i : i + 1, :]
+            mixed = jnp.concatenate(
+                [silu(mixed), jnp.zeros((LANES - batch, key_cols), F32)], axis=0
+            )
+            for p in split3(mixed):
+                keys_t = keys_t + lax.dot_general(
+                    send_hot[i], p, NT, preferred_element_type=F32
+                )
+        keys_send[l] = keys_t.reshape(GROUPS, span, LANES)
+        keys_recv[l, me] = keys_send[l, my_group]
+        if l == 0:
+            pl.semaphore_wait(barrier, n - 1)
+        each(lambda k: key_copy(l, k, me).start())
+
+        big[l][2].wait()
+        big[l][3].wait()
+        big[l][4].wait()
+        gate_in, value_in, step_in = project((wg, wv, ws))
+        value_out[l] = value_in
+        values = value_in * cvw[l, TAPS - 1 : TAPS, :]
+        for k in range(TAPS - 1):
+            values = values + cv[l, k] * cvw[l, k : k + 1, :]
+        values = silu(values)
+        raw = step_in + bias[l : l + 1, :]
+        delta = jnp.maximum(raw, 0.0) + jnp.log1p(jnp.exp(-jnp.abs(raw)))
+        decay = jnp.exp(-delta * rate[l : l + 1, :])
+        skips = jnp.broadcast_to(skip[l : l + 1, :], (8, heads))
+        chan = select_dot(jnp.concatenate([delta, decay, skips], axis=0), head_hot)
+        decay_chan = chan[batch : 2 * batch]
+        skip_chan = chan[2 * batch : 2 * batch + 1]
+        dv = chan[:batch] * values
+        cols[...] = jnp.concatenate(
+            [dv, decay_chan, jnp.zeros((LANES - 2 * batch, chans), F32)], axis=0
+        ).T
+        gate = silu(gate_in)
+        big[l][5].wait()
+
+        each(lambda k: key_copy(l, k, came_from(k)).wait_recv())
+        arrived = keys_recv[l].reshape(n * span, LANES).T[:batch]
+        both = select_dot(arrived, recv_hot)
+        writes = both[:, :entries]
+        reads = both[:, entries:]
+        wbuf[...] = writes
+        rbuf[...] = reads
+        lane_half = iota((8, 2 * entries), 1) // entries
+        sub = iota((8, 2 * entries), 0)
+
+        def query(g, carry):
+            at = pl.ds(pl.multiple_of(8 * g, 8), 8)
+            reads8 = rbuf[at, :]
+            twice = jnp.concatenate([reads8, reads8], axis=1)
+            total = jnp.zeros((8, chans), F32)
+            for p in range(4):
+                left = jnp.where(sub == 2 * p + lane_half, twice, 0.0).astype(BF16)
+                right = jnp.concatenate(
+                    [state[l, 8 * g + 2 * p], state[l, 8 * g + 2 * p + 1]], axis=1
+                ).astype(BF16)
+                total = total + lax.dot_general(left, right, NT, preferred_element_type=F32)
+            qbuf[at, :] = total
+            return carry
+
+        lax.fori_loop(0, groups8, query, 0)
+        through = jnp.sum(writes * reads, axis=1, keepdims=True)
+        mixed_out = decay_chan * qbuf[...] + dv * through + skip_chan * values
+        gated = mixed_out * gate
+        sq_send[l] = jnp.broadcast_to(
+            jnp.sum(gated * gated, axis=1, keepdims=True), (batch, LANES)
+        )
+        for k in range(1, peers):
+            sq_copy(l, k).start()
+        fed = (gated * gg[l : l + 1, :]).astype(BF16)
+        big[l][6].wait()
+        per = 4
+
+        def out_step(t, carry):
+            res = jnp.dot(
+                fed,
+                wo[l, :, pl.ds(pl.multiple_of(t * per * width, per * width), per * width)],
+                preferred_element_type=F32,
+            )
+            for i in range(per):
+                part[t * per + i] = res[:, i * width : (i + 1) * width]
+            return carry
+
+        lax.fori_loop(0, n // per, out_step, 0)
+        for k in range(1, peers):
+            sq_copy(l, k).wait_recv()
+        total = sq_send[l]
+        for k in range(1, peers):
+            total = total + sq_recv[l, k]
+        scale = lax.rsqrt(total / GW + EPS)
+        for j in range(n):
+            rs_send[l, j] = (part[j] * scale[:, :width]).astype(BF16)
+        each(lambda k: rs_copy(l, k, me).start())
+        update_range(l, 0, groups8 // 2)
+        own = part[me] * scale[:, :width]
+        if l == 0:
+            resid = tokens[:, pl.ds(pl.multiple_of(me * width, width), width)]
+        else:
+            resid = hidden[l - 1, me]
+        each(lambda k: rs_copy(l, k, came_from(k)).wait_recv())
+        rs_recv[l, me] = jnp.zeros((batch, width), BF16)
+        sums = [own, jnp.zeros_like(own), jnp.zeros_like(own), jnp.zeros_like(own)]
+        for j in range(n):
+            sums[j % 4] = sums[j % 4] + rs_recv[l, j].astype(F32)
+        update = (sums[0] + sums[1]) + (sums[2] + sums[3])
+        hidden[l, me] = (resid.astype(F32) + update).astype(BF16)
+        each(lambda k: ag_copy(l, k, me).start())
+        update_range(l, groups8 // 2, groups8)
+        each(lambda k: ag_copy(l, k, came_from(k)).wait_recv())
+
+    for j in range(n):
+        tokens_out[:, j * width : (j + 1) * width] = hidden[layers - 1, j]
+    for l in range(layers):
+        def drain(k):
+            key_copy(l, k, me).wait_send()
+            rs_copy(l, k, me).wait_send()
+            ag_copy(l, k, me).wait_send()
+
+        each(drain)
+        for k in range(1, peers):
+            sq_copy(l, k).wait_send()
+        for g in range(groups8):
+            pltpu.make_async_copy(
+                state.at[l, pl.ds(8 * g, 8)],
+                state_out.at[l, pl.ds(8 * g, 8)],
+                out_sem.at[l, g],
+            ).wait()
+
+
+def fused(n, *args):
+    (tokens, norm_gain, w_gate, w_value, w_write, w_read, w_step, step_bias, decay_rate) = args[:9]
+    (skip_gain, cvw, ckw, group_gain, w_out, ssm_state, conv_value, conv_key) = args[9:]
+    layers, batch, chans, entries = ssm_state.shape
+    depth = tokens.shape[1]
+    key_cols = w_write.shape[2]
+    peers = GW // chans
+    span = 2 * (key_cols // GROUPS)
+    width = depth // n
+    operands = list(args[:15]) + [
+        jnp.transpose(conv_value, (0, 2, 1, 3)),
+        jnp.transpose(conv_key, (0, 2, 3, 1, 4)),
+    ]
+    landed = [pltpu.VMEM(a.shape, a.dtype) for a in operands]
+    dma = pltpu.SemaphoreType.DMA
+    hidden, state, value_in, write_in, read_in = pl.pallas_call(
+        functools.partial(kernel, n),
+        out_shape=(
+            jax.ShapeDtypeStruct(tokens.shape, BF16),
+            jax.ShapeDtypeStruct(ssm_state.shape, F32),
+            jax.ShapeDtypeStruct((layers, batch, chans), F32),
+            jax.ShapeDtypeStruct((layers, batch, key_cols), F32),
+            jax.ShapeDtypeStruct((layers, batch, key_cols), F32),
+        ),
+        in_specs=[pl.BlockSpec(memory_space=pl.ANY)] * len(operands),
+        out_specs=(
+            pl.BlockSpec(memory_space=pltpu.VMEM),
+            pl.BlockSpec(memory_space=pl.ANY),
+            pl.BlockSpec(memory_space=pltpu.VMEM),
+            pl.BlockSpec(memory_space=pltpu.VMEM),
+            pl.BlockSpec(memory_space=pltpu.VMEM),
+        ),
+        scratch_shapes=landed
+        + [
+            pltpu.VMEM((layers, n, batch, width), BF16),
+            pltpu.VMEM((batch, depth), BF16),
+            pltpu.VMEM((layers, GROUPS, span, LANES), F32),
+            pltpu.VMEM((layers, n, span, LANES), F32),
+            pltpu.VMEM((layers, batch, LANES), F32),
+            pltpu.VMEM((layers, peers, batch, LANES), F32),
+            pltpu.VMEM((n, batch, width), F32),
+            pltpu.VMEM((layers, n, batch, width), BF16),
+            pltpu.VMEM((layers, n, batch, width), BF16),
+            pltpu.VMEM((chans, LANES), F32),
+            pltpu.VMEM((batch, entries), F32),
+            pltpu.VMEM((batch, entries), F32),
+            pltpu.VMEM((batch, chans), F32),
+            dma((10,)),
+            dma((layers, 7)),
+            dma((layers, batch // 8)),
+            dma((layers, n)),
+            dma((layers, n)),
+            dma((layers, peers)),
+            dma((layers, peers)),
+            dma((layers, n)),
+            dma((layers, n)),
+            dma((layers, n)),
+            dma((layers, n)),
+        ],
+        compiler_params=pltpu.CompilerParams(
+            collective_id=0, has_side_effects=True, vmem_limit_bytes=60 * 1024 * 1024
+        ),
+        name="mixer",
+    )(*operands)
+    value_state = jnp.concatenate([conv_value[:, :, 1:], value_in[:, :, None]], axis=2)
+    fresh = jnp.stack([write_in, read_in], axis=2)[:, :, None]
+    key_state = jnp.concatenate([conv_key[:, :, 1:], fresh], axis=2)
+    return hidden, state, value_state, key_state
+
+
+def dispatch(n, *args):
+    depth = args[0].shape[1]
+    batch, chans = args[14].shape[1:3]
+    own_entries = args[4].shape[2] // GROUPS
+    fits = (
+        depth == n * LANES
+        and 2 * own_entries == 8
+        and chans % LANES == 0
+        and GW % chans == 0
+        and 2 * batch <= LANES
+        and batch % 16 == 0
+    )
+    return fused(n, *args) if fits else per_device(*args)
+
+
 def solution(mesh):
     placed = (
         P(),
@@ -119,7 +616,7 @@
         P(None, None, None, None, "tp"),
     )
     return jax.shard_map(
-        per_device,
+        functools.partial(dispatch, mesh.shape["tp"]),
         mesh=mesh,
         in_specs=placed,
         out_specs=(

time: 487 us -> 89.4 us (0.18)
  waiting for transfers between devices: 250 us -> 0 us
  blocking collectives: 162 us -> 0 us
  Pallas kernels: 0 us -> 68.2 us
  other arithmetic: 35.8 us -> 1.64 us
  matrix products: 18 us -> 0 us
  between operations: 14.5 us -> 0.71 us
  local copies, waits for them, and re-layouts: 5.49 us -> 18.3 us
    psum x2 -> x0, waiting for transfers between devices: 250 us -> none  [per_device(): update = lax.psum(partial_out, 'tp')]
    all_gather x2 -> x0, blocking collectives: 88.7 us -> none  [per_device(): every_group = lax.all_gather(mixed_keys, 'tp', axis=2, tiled=True)]
    psum x2 -> x0, blocking collectives: 73.6 us -> none  [per_device(): square_total = lax.psum(squares, 'tp')]
    pallas_call x0 -> x1, Pallas kernels: none -> 68.2 us  [fused(): pl.pallas_call(functools.partial(kernel, n), out_shape=(jax.ShapeDtypeStr...]
    unnamed x20 -> x17, local copies, waits for them, and re-layouts: 0.08 us -> 18.2 us
    dot_general x22 -> x0, matrix products: 18 us -> none  [the longest x10 9.71 us: project(): jnp.dot(scaled, weight[layer], preferred_element_type=jnp.float32)]
    reduce_sum x8 -> x0, other arithmetic: 14 us -> none  [the longest x2 11 us: per_device(): jnp.sum(state * reads[:, None, :], axis=2) + skip_chan[None] * values]
    add x1 -> x0, other arithmetic: 10.5 us -> none  [per_device(): decay_chan[..., None] * ssm_state[layer]]
  transfers between devices with their start and end apart: 2 -> 0, of which waited for: 2 -> 0; matrix products, arithmetic and copies ran while one was open for 2% -> 0% of each run, Pallas kernels for 0% -> 0%
where the time goes in v1:
time: 89.4 us; the launch traced here: 88.9 us
  Pallas kernels  68.2 us (76%)
  local copies, waits for them, and re-layouts  18.3 us (20%)
  other arithmetic  1.64 us (2%)
    pallas_call x1, Pallas kernels, fused(): pl.pallas_call(functools.partial(kernel, n), out_shape=(jax.ShapeDtypeStr...  68.2 us
    unnamed x17, local copies, waits for them, and re-layouts  18.2 us

profile of v1, /device:TPU:0, one launch (start us, length us, event | category | flops | bytes accessed | tf_op | source)
XLA Modules:
  0.0 88.9 jit_solution(13967638808445175703)
XLA Ops:
  0.6 0.0 copy-start.2
  0.6 0.0 copy-start
  0.7 0.0 copy-start.1
  0.7 2.7 %copy.23.ww_hbm = bf16[2,4096,32]{2,1,0:T(8,128)(2,1)} copy(bf16[2,4096,32]{1,2,0:T(8,128)(2,1)} %param.21) | data formatting | bytes 1048576 | tf_op args[4]
  3.3 2.7 %copy.24.wr_hbm = bf16[2,4096,32]{2,1,0:T(8,128)(2,1)} copy(bf16[2,4096,32]{1,2,0:T(8,128)(2,1)} %param.22) | data formatting | bytes 1048576 | tf_op args[5]
  6.0 0.0 copy-done.2
  6.0 0.6 copy.25.cvw_hbm
  6.6 0.0 copy-done
  6.6 0.7 copy.35
  7.3 0.0 copy-done.1
  7.3 0.7 copy.34
  7.9 0.0 slice-start
  7.9 68.2 %mixer.1 = (bf16[32,4096]{1,0:T(8,128)(2,1)}, f32[2,32,256,128]{3,2,1,0:T(8,128)}, f32[2,32,256]{2,1,0:T(8,128)}, f32[2,32,32]{2,1,0:T(8,128)}, f32[2,32,32]{2,1,0:T(8,128)}) custom-call(bf16[32,4096]{1,0:T(8,128)(2,1)} %tokens_hbm.1, f32[2,4096]{1,0:T(2,128)} %gain_hbm.1, bf16[2,4096,256]{2,1,0:T(8,128)(2,1)} %wg_hbm.1, bf16[2,4096,256]{2,1,0:T(8,128)(2,1)} %wv_hbm.1, ...), custom_call_target="tpu_custom_call" | custom-call | tf_op jit(solution)/shard_map/mixer/pallas_call | solution.py:528
  76.1 0.1 slice.6
  76.2 0.8 pad_maximum_fusion
  77.1 0.8 copy.28
  77.8 0.8 maximum_bitcast_fusion
  78.6 0.0 slice-done
  78.7 0.8 copy.29
  79.4 1.7 %copy.38 = bf16[32,4096]{1,0:T(8,128)(2,1)} copy(bf16[32,4096]{1,0:T(8,128)(2,1)} %get-tuple-element.22) | data formatting | bytes 524288
  81.1 7.8 %copy.39 = f32[2,32,256,128]{3,2,1,0:T(8,128)} copy(f32[2,32,256,128]{3,2,1,0:T(8,128)} %get-tuple-element.23) | data formatting | bytes 16777216
  (3 shorter events, 0.0 us)
Async XLA Ops:
  0.6 5.4 %copy-start.2 = (f32[2,3,256]{2,0,1:T(2,128)S(1)}, f32[2,3,256]{2,0,1:T(2,128)}, u32[]{:S(2)}) copy-start(f32[2,3,256]{2,0,1:T(2,128)} %param.27) | copy-start | bytes 18436
  0.6 6.0 %copy-start = (f32[2,32,2,256]{3,2,1,0:T(2,128)S(1)}, f32[2,32,2,256]{3,2,1,0:T(2,128)}, u32[]{:S(2)}) copy-start(f32[2,32,2,256]{3,2,1,0:T(2,128)} %param.32) | copy-start | bytes 393220
  0.7 6.6 %copy-start.1 = (f32[2,32,2,2,32]{4,3,2,1,0:T(2,128)S(1)}, f32[2,32,2,2,32]{4,3,2,1,0:T(2,128)}, u32[]{:S(2)}) copy-start(f32[2,32,2,2,32]{4,3,2,1,0:T(2,128)} %param.33) | copy-start | bytes 98308
  7.9 70.7 %slice-start = ((f32[2,32,2,2,32]{4,3,2,1,0:T(2,128)}), f32[2,32,1,2,32]{4,3,2,1,0:T(2,128)S(1)}, s32[]{:S(2)}) async-start(f32[2,32,2,2,32]{4,3,2,1,0:T(2,128)} %param.33), calls=%async_computation | async-start | bytes 131072 | tf_op jit(solution)/shard_map/slice | solution.py:579

commit v2 on v1

--- a/solution.py
+++ b/solution.py
@@ -103,6 +103,7 @@
 
 LANES = 128
 TAPS = 3
+VMEM = 67043328
 BF16 = jnp.bfloat16
 F32 = jnp.float32
 NT = (((1,), (1,)), ((), ()))
@@ -150,16 +151,14 @@
     cv_hbm,
     ck_hbm,
     tokens_out,
-    state_out,
+    state,
     value_out,
-    write_out,
-    read_out_ref,
+    key_out,
     tokens,
     gain,
     wg,
     wv,
-    ww,
-    wr,
+    wk,
     ws,
     bias,
     rate,
@@ -168,7 +167,6 @@
     ckw,
     gg,
     wo,
-    state,
     cv,
     ck,
     hidden,
@@ -186,7 +184,6 @@
     qbuf,
     in_small,
     in_big,
-    out_sem,
     key_ss,
     key_rs,
     sq_ss,
@@ -199,7 +196,7 @@
     layers, batch, chans, entries = state.shape
     width = hidden.shape[3]
     depth = tokens.shape[1]
-    key_cols = ww.shape[2]
+    key_cols = wk.shape[1] // 2
     own_entries = key_cols // GROUPS
     span = 2 * own_entries
     heads = bias.shape[1]
@@ -228,8 +225,8 @@
             pltpu.make_async_copy(a.at[l], b.at[l], in_big.at[l, i])
             for i, (a, b) in enumerate(
                 (
-                    (ww_hbm, ww),
-                    (wr_hbm, wr),
+                    (ww_hbm, wk.at[:, :key_cols]),
+                    (wr_hbm, wk.at[:, key_cols:]),
                     (wg_hbm, wg),
                     (wv_hbm, wv),
                     (ws_hbm, ws),
@@ -282,6 +279,13 @@
             hidden.at[l, me], hidden.at[l, slot], ag_ss.at[l, k], ag_rs.at[l, k], to
         )
 
+    buddy = me + 1 - 2 * lax.rem(me, 2)
+
+    def pair_copy(l, k, slot):
+        return remote(
+            hidden.at[l, slot], hidden.at[l, slot], ag_ss.at[l, k], ag_rs.at[l, k], buddy
+        )
+
     def sq_copy(l, k):
         to = first + lax.rem(me - first + k, peers)
         return remote(
@@ -294,6 +298,13 @@
             return carry
 
         lax.fori_loop(1, n, step, 0)
+
+    def halves(body):
+        def step(k, carry):
+            body(2 * k)
+            return carry
+
+        lax.fori_loop(1, n // 2, step, 0)
 
     def came_from(k):
         return lax.rem(me + n - k, n)
@@ -322,11 +333,6 @@
                 turned[:, batch + j : batch + j + 1] * state[l, b]
                 + turned[:, j : j + 1] * writes8[j : j + 1, :]
             )
-        pltpu.make_async_copy(
-            state.at[l, pl.ds(8 * group, 8)],
-            state_out.at[l, pl.ds(8 * group, 8)],
-            out_sem.at[l, group],
-        ).start()
 
     groups8 = batch // 8
 
@@ -370,17 +376,28 @@
 
         big[l][0].wait()
         big[l][1].wait()
-        write_in, read_in = project((ww, wr))
-        write_out[l] = write_in
-        read_out_ref[l] = read_in
+        def key_step(k, acc):
+            at = pl.ds(pl.multiple_of(k * kstep, kstep), kstep)
+            return acc + lax.dot_general(
+                scaled[:, at], wk[l, :, at], NT, preferred_element_type=F32
+            )
+
+        key_in = lax.fori_loop(0, ksteps, key_step, jnp.zeros((batch, 2 * key_cols), F32))
+        key_in = key_in * inv_scale
+        write_in = key_in[:, :key_cols]
+        read_in = key_in[:, key_cols:]
         if l == 0:
             for copy in small[2:]:
                 copy.wait()
+        for i, fresh in enumerate((write_in, read_in)):
+            for k in range(1, TAPS - 1):
+                key_out[l, :, k - 1, i, :] = ck[l, :, k, i, :]
+            key_out[l, :, TAPS - 2, i, :] = fresh
         keys_t = jnp.zeros((2 * key_cols, LANES), F32)
         for i, fresh in enumerate((write_in, read_in)):
             mixed = fresh * ckw[l, TAPS - 1, i : i + 1, :]
             for k in range(TAPS - 1):
-                mixed = mixed + ck[l, k, i] * ckw[l, k, i : i + 1, :]
+                mixed = mixed + ck[l, :, k, i, :] * ckw[l, k, i : i + 1, :]
             mixed = jnp.concatenate(
                 [silu(mixed), jnp.zeros((LANES - batch, key_cols), F32)], axis=0
             )
@@ -398,10 +415,12 @@
         big[l][3].wait()
         big[l][4].wait()
         gate_in, value_in, step_in = project((wg, wv, ws))
-        value_out[l] = value_in
-        values = value_in * cvw[l, TAPS - 1 : TAPS, :]
+        for k in range(1, TAPS - 1):
+            value_out[l, :, k - 1, :] = cv[l, :, k, :]
+        value_out[l, :, TAPS - 2, :] = value_in
+        values = value_in * cvw[TAPS - 1, l : l + 1, :]
         for k in range(TAPS - 1):
-            values = values + cv[l, k] * cvw[l, k : k + 1, :]
+            values = values + cv[l, :, k, :] * cvw[k, l : l + 1, :]
         values = silu(values)
         raw = step_in + bias[l : l + 1, :]
         delta = jnp.maximum(raw, 0.0) + jnp.log1p(jnp.exp(-jnp.abs(raw)))
@@ -487,9 +506,17 @@
             sums[j % 4] = sums[j % 4] + rs_recv[l, j].astype(F32)
         update = (sums[0] + sums[1]) + (sums[2] + sums[3])
         hidden[l, me] = (resid.astype(F32) + update).astype(BF16)
-        each(lambda k: ag_copy(l, k, me).start())
+        pair_copy(l, 1, me).start()
+        halves(lambda k: ag_copy(l, k, me).start())
         update_range(l, groups8 // 2, groups8)
-        each(lambda k: ag_copy(l, k, came_from(k)).wait_recv())
+
+        def forward(k):
+            ag_copy(l, k, came_from(k)).wait_recv()
+            pair_copy(l, k + 1, came_from(k)).start()
+
+        halves(forward)
+        pair_copy(l, 1, buddy).wait_recv()
+        halves(lambda k: pair_copy(l, k + 1, lax.rem(buddy + n - k, n)).wait_recv())
 
     for j in range(n):
         tokens_out[:, j * width : (j + 1) * width] = hidden[layers - 1, j]
@@ -497,17 +524,17 @@
         def drain(k):
             key_copy(l, k, me).wait_send()
             rs_copy(l, k, me).wait_send()
+
+        each(drain)
+        pair_copy(l, 1, me).wait_send()
+
+        def drain_pair(k):
             ag_copy(l, k, me).wait_send()
-
-        each(drain)
+            pair_copy(l, k + 1, came_from(k)).wait_send()
+
+        halves(drain_pair)
         for k in range(1, peers):
             sq_copy(l, k).wait_send()
-        for g in range(groups8):
-            pltpu.make_async_copy(
-                state.at[l, pl.ds(8 * g, 8)],
-                state_out.at[l, pl.ds(8 * g, 8)],
-                out_sem.at[l, g],
-            ).wait()
 
 
 def fused(n, *args):
@@ -519,25 +546,25 @@
     peers = GW // chans
     span = 2 * (key_cols // GROUPS)
     width = depth // n
-    operands = list(args[:15]) + [
-        jnp.transpose(conv_value, (0, 2, 1, 3)),
-        jnp.transpose(conv_key, (0, 2, 3, 1, 4)),
-    ]
+    operands = list(args)
+    operands[4] = jnp.swapaxes(w_write, 1, 2)
+    operands[5] = jnp.swapaxes(w_read, 1, 2)
+    operands[10] = jnp.swapaxes(cvw, 0, 1)
     landed = [pltpu.VMEM(a.shape, a.dtype) for a in operands]
+    landed[4:6] = [pltpu.VMEM((layers, 2 * key_cols, depth), BF16)]
+    del landed[13]
     dma = pltpu.SemaphoreType.DMA
-    hidden, state, value_in, write_in, read_in = pl.pallas_call(
+    hidden, state, value_state, key_state = pl.pallas_call(
         functools.partial(kernel, n),
         out_shape=(
             jax.ShapeDtypeStruct(tokens.shape, BF16),
-            jax.ShapeDtypeStruct(ssm_state.shape, F32),
-            jax.ShapeDtypeStruct((layers, batch, chans), F32),
-            jax.ShapeDtypeStruct((layers, batch, key_cols), F32),
-            jax.ShapeDtypeStruct((layers, batch, key_cols), F32),
+            pltpu.VMEM(ssm_state.shape, F32),
+            jax.ShapeDtypeStruct(conv_value.shape, F32),
+            jax.ShapeDtypeStruct(conv_key.shape, F32),
         ),
-        in_specs=[pl.BlockSpec(memory_space=pl.ANY)] * len(operands),
+        in_specs=[pl.BlockSpec(memory_space=pltpu.HBM)] * len(operands),
         out_specs=(
             pl.BlockSpec(memory_space=pltpu.VMEM),
-            pl.BlockSpec(memory_space=pl.ANY),
             pl.BlockSpec(memory_space=pltpu.VMEM),
             pl.BlockSpec(memory_space=pltpu.VMEM),
             pl.BlockSpec(memory_space=pltpu.VMEM),
@@ -559,7 +586,6 @@
             pltpu.VMEM((batch, chans), F32),
             dma((10,)),
             dma((layers, 7)),
-            dma((layers, batch // 8)),
             dma((layers, n)),
             dma((layers, n)),
             dma((layers, peers)),
@@ -570,13 +596,10 @@
             dma((layers, n)),
         ],
         compiler_params=pltpu.CompilerParams(
-            collective_id=0, has_side_effects=True, vmem_limit_bytes=60 * 1024 * 1024
+            collective_id=0, has_side_effects=True, vmem_limit_bytes=VMEM - ssm_state.size * 4 - 768 * 1024
         ),
         name="mixer",
     )(*operands)
-    value_state = jnp.concatenate([conv_value[:, :, 1:], value_in[:, :, None]], axis=2)
-    fresh = jnp.stack([write_in, read_in], axis=2)[:, :, None]
-    key_state = jnp.concatenate([conv_key[:, :, 1:], fresh], axis=2)
     return hidden, state, value_state, key_state
 
 
@@ -591,6 +614,7 @@
         and GW % chans == 0
         and 2 * batch <= LANES
         and batch % 16 == 0
+        and n % 2 == 0
     )
     return fused(n, *args) if fits else per_device(*args)
 

time: 89.4 us -> 72.7 us (0.81)
  local copies, waits for them, and re-layouts: 18.3 us -> 5.43 us
  Pallas kernels: 68.2 us -> 65.8 us
  other arithmetic: 1.64 us -> 0 us
    unnamed x17 -> x10, local copies, waits for them, and re-layouts: 18.2 us -> 5.43 us
    pallas_call x1, Pallas kernels: 68.2 us -> 65.8 us  [fused(): pl.pallas_call(functools.partial(kernel, n), out_shape=(jax.ShapeDtypeStr...]
where the time goes in v2:
time: 72.7 us; the launch traced here: 71.9 us
  Pallas kernels  65.8 us (91%)
  local copies, waits for them, and re-layouts  5.43 us (7%)
    pallas_call x1, Pallas kernels, fused(): pl.pallas_call(functools.partial(kernel, n), out_shape=(jax.ShapeDtypeStr...  65.8 us
    unnamed x10, local copies, waits for them, and re-layouts  5.43 us

profile of v2, /device:TPU:0, one launch (start us, length us, event | category | flops | bytes accessed | tf_op | source)
XLA Modules:
  0.0 71.9 jit_solution(10906734361440390479)
XLA Ops:
  0.6 65.8 %mixer.1 = (bf16[32,4096]{1,0:T(8,128)(2,1)}, f32[2,32,256,128]{3,2,1,0:T(8,128)S(1)}, f32[2,32,2,256]{3,2,1,0:T(2,128)}, f32[2,32,2,2,32]{4,3,2,1,0:T(2,128)}) custom-call(bf16[32,4096]{1,0:T(8,128)(2,1)} %tokens_hbm.1, f32[2,4096]{1,0:T(2,128)} %gain_hbm.1, bf16[2,4096,256]{2,1,0:T(8,128)(2,1)} %wg_hbm.1, bf16[2,4096,256]{2,1,0:T(8,128)(2,1)} %wv_hbm.1, ...), custom_call_target="tpu_custom_call" | custom-call | tf_op jit(solution)/shard_map/mixer/pallas_call | solution.py:557
  66.5 0.0 copy-start
  66.5 0.0 copy-start.2
  66.5 0.0 copy-start.1
  66.5 3.4 %copy.25 = f32[2,32,256,128]{3,2,1,0:T(8,128)} copy(f32[2,32,256,128]{3,2,1,0:T(8,128)S(1)} %get-tuple-element.5) | data formatting | bytes 16777216
  69.9 0.0 copy-done
  69.9 0.7 copy.26
  70.6 0.0 copy-done.2
  70.6 0.7 copy.27
  71.2 0.0 copy-done.1
  71.3 0.7 copy.28
Async XLA Ops:
  66.5 3.4 %copy-start = (bf16[32,4096]{1,0:T(8,128)(2,1)S(1)}, bf16[32,4096]{1,0:T(8,128)(2,1)}, u32[]{:S(2)}) copy-start(bf16[32,4096]{1,0:T(8,128)(2,1)} %get-tuple-element.12) | copy-start | bytes 786436
  66.5 4.1 %copy-start.2 = (f32[2,32,2,256]{3,2,1,0:T(2,128)S(1)}, f32[2,32,2,256]{3,2,1,0:T(2,128)}, u32[]{:S(2)}) copy-start(f32[2,32,2,256]{3,2,1,0:T(2,128)} %get-tuple-element.14) | copy-start | bytes 393220
  66.5 4.8 %copy-start.1 = (f32[2,32,2,2,32]{4,3,2,1,0:T(2,128)S(1)}, f32[2,32,2,2,32]{4,3,2,1,0:T(2,128)}, u32[]{:S(2)}) copy-start(f32[2,32,2,2,32]{4,3,2,1,0:T(2,128)} %get-tuple-element.15) | copy-start | bytes 98308
